TPU v7x, 1024 devices: a whole 8x8x8 slice. The times are simulated.
1024 devices in a mesh: rep: 8 (over y), fs: 32 (over z, x_hi), tp: 4 (over x_lo, core).
Axes of the slice: x: 8 (x_hi: 4, x_lo: 2; x = x_hi * 2 + x_lo), y: 8, z: 8, core: 2. Of those that a mesh axis runs over, the one named last changes fastest.
Arguments:
- tokens: bfloat16 [256, 192, 2048], P(('rep', 'fs'), None, 'tp'), may hold values from -40 to 40
- ff_first: bfloat16 [2048, 2048], P('fs', 'tp'), may hold values from -0.125 to 0.125
- ff_second: bfloat16 [2048, 2048], P('fs', 'tp'), may hold values from -0.125 to 0.125
- ff_down: bfloat16 [2048, 2048], P('fs', 'tp'), may hold values from -0.125 to 0.125
- mix_stream: bfloat16 [2048, 2048], P('fs', 'tp'), may hold values from -0.125 to 0.125
- mix_gate: bfloat16 [2048, 2048], P('fs', 'tp'), may hold values from -0.125 to 0.125
- mix_down: bfloat16 [2048, 2048], P('fs', 'tp'), may hold values from -0.125 to 0.125
- gain_one: float32 [2048], P('tp'), may hold values from 0.1 to 1.9
- gain_two: float32 [2048], P('tp'), may hold values from 0.1 to 1.9
- gain_three: float32 [2048], P('tp'), may hold values from 0.1 to 1.9
Outputs:
- layer_out: bfloat16 [256, 192, 2048], P(('rep', 'fs'), None, 'tp')
All inputs are finite; a program needn't handle non-finite values.
Results may differ from a plain program's by a relative error of at most 0.01.
Values may be sent and summed in bfloat16 or wider, within the bound.
No kernel may reach another device: no remote copies, remote signals or barrier semaphores. Data moves between devices by JAX's collectives and lax.ppermute only.
A program may use at most 64 MiB of HBM per device.

v0:
```python
import jax
import jax.numpy as jnp
from jax import lax
from jax.experimental import pallas as pl
from jax.experimental.pallas import tpu as pltpu
from jax.sharding import Mesh
from jax.sharding import PartitionSpec as P


alpha_scale = 2.0**0.5
norm_eps = 1e-05
BF = jnp.bfloat16
F32 = jnp.float32

SEQ = 192
D = 2048
LOC = 512
ROWS = 208
NZ = 8
NX = 4
KB = 256


def _dot(a, b):
    return jnp.dot(a, b, preferred_element_type=F32)


def _product_whole(h_ref, w_ref, col, width, wait=None):
    acc = None
    for k in range(NZ):
        if wait is not None:
            wait[k].wait()
        rows = slice(k * KB, (k + 1) * KB)
        part = _dot(h_ref[:, rows], w_ref[rows, col : col + width])
        acc = part if acc is None else acc + part
    return acc


NEAR = (0, 1, 7, 2)
FAR = (3, 6, 4, 5)


def _product_ring(h_ref, near, far, col, width, wait=None):
    y = lax.axis_index("rep")
    z = lax.axis_index("z")
    acc = None
    for i, k in enumerate(NEAR + FAR):
        if wait is not None and i >= 4:
            wait[i - 4].wait()
        block = near[i] if i < 4 else far.at[i - 4]
        zb = lax.rem(z + y + k, NZ)
        h = h_ref[:, pl.ds(pl.multiple_of(zb * KB, KB), KB)]
        part = _dot(h, block[:, col : col + width])
        acc = part if acc is None else acc + part
    return acc


def _tp_index():
    return lax.axis_index("xl") * 2 + lax.axis_index("co")


def _gain(gain_ref, row, j):
    at = slice(j * LOC, (j + 1) * LOC)
    term = lambda i: gain_ref[row + i : row + i + 1, at].astype(F32)
    return term(0) + term(1) + term(2)


def _normed(pay_ref, gain_ref, row, h_ref):
    width = 2 * 128
    token = lax.broadcasted_iota(jnp.int32, (SEQ, width), 0)
    lane = lax.broadcasted_iota(jnp.int32, (SEQ, width), 1)
    cents, sums = [], None
    for j in range(4):
        zc = pay_ref[:SEQ, j * LOC : (j + 1) * LOC].astype(F32)
        terms = pay_ref[SEQ:, j * LOC : j * LOC + width].astype(F32)
        across = jnp.sum(terms, axis=0, keepdims=True)
        cent = jnp.sum(jnp.where(token == lane, across, 0.0), axis=1, keepdims=True)
        s = jnp.sum(zc, axis=1, keepdims=True) + LOC * cent
        sums = s if sums is None else sums + s
        cents.append(cent)
    mean = sums / D
    var = None
    for j in range(4):
        zc = pay_ref[:SEQ, j * LOC : (j + 1) * LOC].astype(F32)
        dev = zc + (cents[j] - mean)
        v = jnp.sum(dev * dev, axis=1, keepdims=True)
        var = v if var is None else var + v
    scale = lax.rsqrt(var / D + norm_eps)
    for j in range(4):
        zc = pay_ref[:SEQ, j * LOC : (j + 1) * LOC].astype(F32)
        dev = zc + (cents[j] - mean)
        g = _gain(gain_ref, row, j)
        h_ref[:, j * LOC : (j + 1) * LOC] = (dev * scale * g).astype(BF)


def _payload(total, out_ref):
    cent = jnp.sum(total, axis=1, keepdims=True) / LOC
    out_ref[:SEQ] = (total - cent).astype(BF)
    token = lax.broadcasted_iota(jnp.int32, (SEQ, LOC), 0)
    lane = lax.broadcasted_iota(jnp.int32, (SEQ, LOC), 1)
    across = jnp.sum(jnp.where(token == lane, cent, 0.0), axis=0, keepdims=True)
    hi, mid, low = _terms(across)
    line = lax.broadcasted_iota(jnp.int32, (ROWS - SEQ, LOC), 0)
    terms = jnp.where(line == 0, hi, jnp.where(line == 1, mid, jnp.where(line == 2, low, 0.0)))
    out_ref[SEQ:] = terms.astype(BF)


def _own(h_ref):
    return h_ref[:, pl.ds(pl.multiple_of(_tp_index() * LOC, LOC), LOC)]


def _ff_in_first(tok_ref, w_ref, out_ref, w, sems):
    copies = [[], []]
    for part, cols in enumerate((slice(0, 2 * LOC), slice(2 * LOC, 3 * LOC))):
        for k in range(NZ):
            at = (slice(k * KB, (k + 1) * KB), cols)
            copies[part].append(pltpu.make_async_copy(w_ref.at[at], w.at[at], sems.at[part, k]))
            copies[part][k].start()
    both = _product_whole(tok_ref.at[:SEQ], w, 0, 2 * LOC, copies[0])
    out_ref[...] = (jax.nn.silu(both[:, :LOC]) * both[:, LOC:]).astype(BF)
    for copy in copies[1]:
        copy.wait()


def _ff_in_normed(pay_ref, gain_ref, w_ref, out_ref, own_ref, h_ref):
    _normed(pay_ref, gain_ref, 3, h_ref)
    own_ref[...] = _own(h_ref)
    both = _product_whole(h_ref, w_ref, 0, 2 * LOC)
    out_ref[...] = (jax.nn.silu(both[:, :LOC]) * both[:, LOC:]).astype(BF)


def _ff_down(hid_ref, own_ref, w_ref, out_ref):
    acc = _product_whole(hid_ref, w_ref, 2 * LOC, LOC)
    _payload(alpha_scale * own_ref[...].astype(F32) + 0.5 * acc, out_ref)


def _mix_down(hid_ref, own_ref, *rest):
    near, (far_ref, out_ref) = rest[:4], rest[4:]
    acc = _product_ring(hid_ref, near, far_ref, 2 * LOC, LOC)
    _payload(alpha_scale * own_ref[...].astype(F32) + acc, out_ref)


def _down_last(hid_ref, own_ref, w_ref, out_ref, stat_ref):
    acc = _product_whole(hid_ref, w_ref, 2 * LOC, LOC)
    total = alpha_scale * own_ref[...].astype(F32) + 0.5 * acc
    out_ref[...] = total
    cent = jnp.sum(total, axis=1, keepdims=True) / LOC
    dev = total - cent
    square = jnp.sum(dev * dev, axis=1, keepdims=True)
    lane = lax.broadcasted_iota(jnp.int32, (SEQ, 128), 1)
    stat_ref[...] = jnp.where(lane == 0, cent, jnp.where(lane == 1, square, 0.0))


def _mix_in(pay_ref, gain_ref, *rest):
    near, blocks, (out_ref, own_ref, far_ref, h_ref, sems) = rest[:4], rest[4:NZ], rest[NZ:]
    copies = [pltpu.make_async_copy(blocks[i], far_ref.at[i], sems.at[i]) for i in range(4)]
    for copy in copies:
        copy.start()
    _normed(pay_ref, gain_ref, 0, h_ref)
    own_ref[...] = _own(h_ref)
    both = _product_ring(h_ref, near, far_ref, 0, 2 * LOC, copies)
    stream = both[:, :LOC].astype(BF)
    gate = both[:, LOC:]
    window = lax.shift_left(jnp.int32(2), _tp_index())
    later = lax.broadcasted_iota(jnp.int32, (SEQ, SEQ), 0)
    earlier = lax.broadcasted_iota(jnp.int32, (SEQ, SEQ), 1)
    offset = later - earlier
    band = jnp.where((offset >= 0) & (offset < window), 1.0, 0.0).astype(BF)
    sums = _dot(band, stream)
    row = lax.broadcasted_iota(jnp.int32, (SEQ, 1), 0)
    counts = jnp.minimum(row + 1, window).astype(F32)
    pooled = sums / counts - stream.astype(F32)
    out_ref[...] = (pooled * jax.nn.silu(gate)).astype(BF)


def _call(kernel, outs, scratch, flops, args, in_hbm=(), limit_mib=6):
    full = pl.BlockSpec(memory_space=pltpu.VMEM)
    far = pl.BlockSpec(memory_space=pltpu.HBM)
    args_bytes = sum(a.size * a.dtype.itemsize for a in (*args, *in_hbm))
    return pl.pallas_call(
        kernel,
        out_shape=outs,
        in_specs=[full] * len(args) + [far] * len(in_hbm),
        out_specs=jax.tree.map(lambda _: full, outs),
        scratch_shapes=scratch,
        cost_estimate=pl.CostEstimate(
            flops=flops, bytes_accessed=args_bytes, transcendentals=0
        ),
        compiler_params=pltpu.CompilerParams(vmem_limit_bytes=limit_mib * 1024 * 1024),
    )(*args, *in_hbm)


def _terms(row):
    hi = row.astype(BF).astype(F32)
    mid = (row - hi).astype(BF).astype(F32)
    return hi, mid, row - hi - mid


def _pack(tok_ref, one_ref, two_ref, out_ref):
    out_ref[:SEQ] = tok_ref[...]
    line = lax.broadcasted_iota(jnp.int32, (ROWS - SEQ, LOC), 0)
    below = jnp.zeros((ROWS - SEQ, LOC), F32)
    for i, term in enumerate(_terms(one_ref[...]) + _terms(two_ref[...])):
        below = jnp.where(line == i, term, below)
    out_ref[SEQ:] = below.astype(BF)


def _sds(cols, dtype=BF, rows=SEQ):
    return jax.ShapeDtypeStruct((rows, cols), dtype)


ONE = 2 * SEQ * D * LOC


def _shift(value, axis, by):
    n = lax.axis_size(axis)
    return lax.ppermute(value, axis, [(i, (i + by) % n) for i in range(n)])


def _diagonal(value):
    pairs = [(y * NZ + (z + y) % NZ, y * NZ + z) for y in range(8) for z in range(NZ)]
    return lax.ppermute(value, ("rep", "z"), pairs)


def _cat(*values, axis=1):
    return jnp.concatenate(values, axis=axis)


def _over_xh(value):
    return lax.all_gather(value, "xh", axis=0, tiled=True)


def _y_ring(block):
    blocks = [None] * 8
    blocks[0] = block
    up = down = block
    for s in range(1, 5):
        down = _shift(down, "rep", -1)
        blocks[s] = down
        if s < 4:
            up = _shift(up, "rep", 1)
            blocks[8 - s] = up
    return blocks


def _whole(local_rows):
    return lax.all_gather(local_rows, ("xl", "co"), axis=1, tiled=True)


def shards(
    tokens, ff_first, ff_second, ff_down, mix_stream, mix_gate, mix_down, gain_one, gain_two, gain_three
):
    tok = tokens[0]
    diag = _diagonal(_cat(mix_stream, mix_gate, mix_down))
    x1 = _over_xh(_cat(ff_first, ff_second, ff_down))
    w_ff = lax.all_gather(x1, "z", axis=0, tiled=True)
    ring = _y_ring(_over_xh(diag))

    block = _call(_pack, _sds(LOC, rows=ROWS), [], 0, (tok, gain_one[None], gain_two[None]))
    whole = _whole(block)

    gains = whole[SEQ:]
    two = (_sds(LOC), _sds(LOC))
    h_scratch = [pltpu.VMEM((SEQ, D), BF)]

    outs = (_sds(LOC), _sds(3 * LOC, rows=D))
    sems = [pltpu.SemaphoreType.DMA((2, NZ))]
    hidden, w_ff = _call(_ff_in_first, outs, sems, 2 * ONE, (whole,), (w_ff,), 44)
    wide = _whole(hidden)
    pay = _call(_ff_down, _sds(LOC, rows=ROWS), [], ONE, (wide, tok, w_ff))

    wide = _whole(pay)
    near, far = [ring[k] for k in NEAR], [ring[k] for k in FAR]
    outs = (*two, jax.ShapeDtypeStruct((4, KB, 3 * LOC), BF))
    scratch = h_scratch + [pltpu.SemaphoreType.DMA((4,))]
    gated, first, far = _call(_mix_in, outs, scratch, 2 * ONE, (wide, gains, *near), far, 6)
    wide = _whole(gated)
    pay = _call(_mix_down, _sds(LOC, rows=ROWS), [], ONE, (wide, first, *near, far))

    wide = _whole(pay)
    hidden, second = _call(_ff_in_normed, two, h_scratch, 2 * ONE, (wide, gains, w_ff))
    wide = _whole(hidden)
    sums = (_sds(LOC, F32), _sds(128, F32))
    total, stats = _call(_down_last, sums, [], ONE, (wide, second, w_ff))

    every = lax.all_gather(stats[:, :2].T, ("xl", "co"), axis=0, tiled=False)
    cents, squares = every[:, 0], every[:, 1]
    mean = jnp.mean(cents, axis=0)
    var = (jnp.sum(squares, axis=0) + LOC * jnp.sum((cents - mean) ** 2, axis=0)) / D
    out = (total - mean[:, None]) * lax.rsqrt(var + norm_eps)[:, None] * gain_three[None, :]
    return out.astype(BF)[None]


def solution(mesh):
    fine = Mesh(mesh.devices.reshape(8, NZ, NX, 2, 2), ("rep", "z", "xh", "xl", "co"))
    rows, cols = ("z", "xh"), ("xl", "co")
    placed = (P(("rep", "z", "xh"), None, cols),) + (P(rows, cols),) * 6 + (P(cols),) * 3
    return jax.shard_map(
        shards, mesh=fine, in_specs=placed, out_specs=P(("rep", "z", "xh"), None, cols), check_vma=False
    )
```

profile of v0, /device:TPU:129, one launch (start us, length us, event | category | flops | bytes accessed | tf_op | source)
XLA Modules:
  0.0 218.6 jit_solution(3778641655627331127)
XLA Ops:
  6.5 0.9 pad_maximum_fusion
  7.5 20.0 %all_gather.34 = bf16[256,1536]{1,0:T(8,128)(2,1)} all-gather(bf16[64,1536]{1,0:T(8,128)(2,1)S(1)} %pad_maximum_fusion), channel_id=1, replica_groups=mesh['rep'=8,'z'=8,'xh'=4,'xl'=2,'co'=2] {'xh'}, dimensions={0}, use_global_device_ids=true | all-gather | bytes 983040 | tf_op jit(solution)/shard_map/all_gather | solution.py:230
  27.5 0.9 pad_maximum_fusion.1
  29.1 17.4 %all_gather.38.rest_0_ = bf16[256,1536]{1,0:T(8,128)(2,1)S(1)} all-gather(bf16[64,1536]{1,0:T(8,128)(2,1)S(1)} %collective-permute-done), channel_id=1, replica_groups=mesh['rep'=8,'z'=8,'xh'=4,'xl'=2,'co'=2] {'xh'}, dimensions={0}, use_global_device_ids=true | all-gather | bytes 983040 | tf_op jit(solution)/shard_map/all_gather | solution.py:230
  46.5 12.9 %collective-permute-start.1 = (bf16[256,1536]{1,0:T(8,128)(2,1)S(1)}, bf16[256,1536]{1,0:T(8,128)(2,1)S(1)}, u32[]{:S(2)}, u32[]{:S(2)}) collective-permute-start(bf16[256,1536]{1,0:T(8,128)(2,1)S(1)} %all_gather.38.rest_0_), channel_id=1, source_target_pairs={{0,896},{128,0},{256,128},{384,256},{512,384},{640,512},{768,640},... | collective-permute-start | bytes 2359304 | tf_op jit(solution)/shard_map/ppermute | solution.py:217
  59.4 1.9 collective-permute-start.2
  61.4 10.1 %collective-permute-done.1.rest_1_ = bf16[256,1536]{1,0:T(8,128)(2,1)S(1)} collective-permute-done((bf16[256,1536]{1,0:T(8,128)(2,1)S(1)}, bf16[256,1536]{1,0:T(8,128)(2,1)S(1)}, u32[]{:S(2)}, u32[]{:S(2)}) %collective-permute-start.1) | collective-permute-done | bytes 786464 | tf_op jit(solution)/shard_map/ppermute | solution.py:217
  71.4 8.4 %collective-permute-start.3 = (bf16[256,1536]{1,0:T(8,128)(2,1)S(1)}, bf16[256,1536]{1,0:T(8,128)(2,1)S(1)}, u32[]{:S(2)}, u32[]{:S(2)}) collective-permute-start(bf16[256,1536]{1,0:T(8,128)(2,1)S(1)} %collective-permute-done.1.rest_1_), channel_id=1, source_target_pairs={{0,896},{128,0},{256,128},{384,256},{512,384},{640,512},{768,640},... | collective-permute-start | bytes 2359304 | tf_op jit(solution)/shard_map/ppermute | solution.py:217
  80.3 8.4 %collective-permute-start.5 = (bf16[256,1536]{1,0:T(8,128)(2,1)S(1)}, bf16[256,1536]{1,0:T(8,128)(2,1)}, u32[]{:S(2)}, u32[]{:S(2)}) collective-permute-start(bf16[256,1536]{1,0:T(8,128)(2,1)S(1)} %collective-permute-done.2.rest_2_), channel_id=1, source_target_pairs={{0,128},{128,256},{256,384},{384,512},{512,640},{640,768},{768,896... | collective-permute-start | bytes 2359304 | tf_op jit(solution)/shard_map/ppermute | solution.py:217
  88.7 12.2 %collective-permute-done.3.rest_3_ = bf16[256,1536]{1,0:T(8,128)(2,1)S(1)} collective-permute-done((bf16[256,1536]{1,0:T(8,128)(2,1)S(1)}, bf16[256,1536]{1,0:T(8,128)(2,1)S(1)}, u32[]{:S(2)}, u32[]{:S(2)}) %collective-permute-start.3) | collective-permute-done | bytes 786464 | tf_op jit(solution)/shard_map/ppermute | solution.py:217
  100.9 14.6 %collective-permute-start.4 = (bf16[256,1536]{1,0:T(8,128)(2,1)S(1)}, bf16[256,1536]{1,0:T(8,128)(2,1)}, u32[]{:S(2)}, u32[]{:S(2)}) collective-permute-start(bf16[256,1536]{1,0:T(8,128)(2,1)S(1)} %collective-permute-done.3.rest_3_), channel_id=1, source_target_pairs={{0,896},{128,0},{256,128},{384,256},{512,384},{640,512},{768,640},... | collective-permute-start | bytes 2359304 | tf_op jit(solution)/shard_map/ppermute | solution.py:217
  115.5 0.9 copy-done
  116.4 0.9 copy-done.2
  117.3 0.7 copy-done.4
  118.0 0.7 copy-done.5
  118.7 1.9 collective-permute-start.7
  120.7 8.1 %collective-permute-done.4.rest_4_ = bf16[256,1536]{1,0:T(8,128)(2,1)} collective-permute-done((bf16[256,1536]{1,0:T(8,128)(2,1)S(1)}, bf16[256,1536]{1,0:T(8,128)(2,1)}, u32[]{:S(2)}, u32[]{:S(2)}) %collective-permute-start.4) | collective-permute-done | bytes 786464 | tf_op jit(solution)/shard_map/ppermute | solution.py:217
  128.8 5.4 %collective-permute-start.6 = (bf16[256,1536]{1,0:T(8,128)(2,1)}, bf16[256,1536]{1,0:T(8,128)(2,1)}, u32[]{:S(2)}, u32[]{:S(2)}) collective-permute-start(bf16[256,1536]{1,0:T(8,128)(2,1)} %collective-permute-done.4.rest_4_), channel_id=1, source_target_pairs={{0,896},{128,0},{256,128},{384,256},{512,384},{640,512},{768,640},... | collective-permute-start | bytes 2359304 | tf_op jit(solution)/shard_map/ppermute | solution.py:217
  134.2 17.1 %all_gather.33.tok_ref = bf16[208,2048]{1,0:T(8,128)(2,1)S(1)} all-gather(bf16[208,512]{1,0:T(8,128)(2,1)S(1)} %shard_map.100), channel_id=1, replica_groups=mesh['rep'=8,'z'=8,'xh'=4,'xl'=2,'co'=2] {'xl','co'}, dimensions={1}, use_global_device_ids=true | all-gather | bytes 1064960 | tf_op jit(solution)/shard_map/all_gather | solution.py:247
  151.3 2.9 %shard_map.101 = (bf16[192,512]{1,0:T(8,128)(2,1)S(1)}, bf16[2048,1536]{1,0:T(8,128)(2,1)S(1)}) custom-call(bf16[208,2048]{1,0:T(8,128)(2,1)S(1)} %all_gather.33.tok_ref, bf16[2048,1536]{1,0:T(8,128)(2,1)} %all-gather.4.cloned.1.call-done.w_ref), custom_call_target="tpu_custom_call" | custom-call | flops 805306368 | bytes 7143424 | tf_op jit(solution)/shard_map/pallas_call | solution.py:180
  154.2 8.8 %all_gather.36.hid_ref = bf16[192,2048]{1,0:T(8,128)(2,1)S(1)} all-gather(bf16[192,512]{1,0:T(8,128)(2,1)S(1)} %get-tuple-element.14), channel_id=1, replica_groups=mesh['rep'=8,'z'=8,'xh'=4,'xl'=2,'co'=2] {'xl','co'}, dimensions={1}, use_global_device_ids=true | all-gather | bytes 983040 | tf_op jit(solution)/shard_map/all_gather | solution.py:247
  163.1 0.7 shard_map.102
  163.8 9.1 %all_gather.37.pay_ref = bf16[208,2048]{1,0:T(8,128)(2,1)S(1)} all-gather(bf16[208,512]{1,0:T(8,128)(2,1)S(1)} %shard_map.102), channel_id=1, replica_groups=mesh['rep'=8,'z'=8,'xh'=4,'xl'=2,'co'=2] {'xl','co'}, dimensions={1}, use_global_device_ids=true | all-gather | bytes 1064960 | tf_op jit(solution)/shard_map/all_gather | solution.py:247
  172.9 3.2 %shard_map.103 = (bf16[192,512]{1,0:T(8,128)(2,1)S(1)}, bf16[192,512]{1,0:T(8,128)(2,1)S(1)}, bf16[4,256,1536]{2,1,0:T(8,128)(2,1)S(1)}) custom-call(bf16[208,2048]{1,0:T(8,128)(2,1)S(1)} %all_gather.37.pay_ref, bf16[16,2048]{1,0:T(8,128)(2,1)S(1)} %slice.16.gain_ref, bf16[256,1536]{1,0:T(8,128)(2,1)S(1)} %all_gather.38.rest_0_, ...), custom_call_target="tpu_custom_call" | custom-call | flops 805306368 | bytes 7208960 | tf_op jit(solution)/shard_map/pallas_call | solution.py:180
  176.1 8.7 %all_gather.39.hid_ref = bf16[192,2048]{1,0:T(8,128)(2,1)S(1)} all-gather(bf16[192,512]{1,0:T(8,128)(2,1)S(1)} %get-tuple-element.16), channel_id=1, replica_groups=mesh['rep'=8,'z'=8,'xh'=4,'xl'=2,'co'=2] {'xl','co'}, dimensions={1}, use_global_device_ids=true | all-gather | bytes 983040 | tf_op jit(solution)/shard_map/all_gather | solution.py:247
  184.8 0.7 shard_map.104
  185.5 9.1 %all_gather.40.pay_ref = bf16[208,2048]{1,0:T(8,128)(2,1)S(1)} all-gather(bf16[208,512]{1,0:T(8,128)(2,1)S(1)} %shard_map.104), channel_id=1, replica_groups=mesh['rep'=8,'z'=8,'xh'=4,'xl'=2,'co'=2] {'xl','co'}, dimensions={1}, use_global_device_ids=true | all-gather | bytes 1064960 | tf_op jit(solution)/shard_map/all_gather | solution.py:247
  194.5 1.6 shard_map.105
  196.1 8.7 %all_gather.41.hid_ref = bf16[192,2048]{1,0:T(8,128)(2,1)S(1)} all-gather(bf16[192,512]{1,0:T(8,128)(2,1)S(1)} %get-tuple-element.19), channel_id=1, replica_groups=mesh['rep'=8,'z'=8,'xh'=4,'xl'=2,'co'=2] {'xl','co'}, dimensions={1}, use_global_device_ids=true | all-gather | bytes 983040 | tf_op jit(solution)/shard_map/all_gather | solution.py:247
  204.9 0.7 shard_map.106
  205.7 5.2 %all-gather.1 = f32[4,2,192]{2,1,0:T(2,128)S(1)} all-gather(f32[1,2,192]{2,1,0:T(2,128)S(1)} %copy.11), channel_id=2, replica_groups=mesh['rep'=8,'z'=8,'xh'=4,'xl'=2,'co'=2] {'xl','co'}, dimensions={0}, use_global_device_ids=true | all-gather | bytes 7680 | tf_op jit(solution)/shard_map/all_gather | solution.py:286
  211.0 0.8 fusion
  (27 shorter events, 1.4 us)
Async XLA Ops:
  6.5 144.8 %all-gather.4.cloned.1.call-start = ((), (), s32[]{:S(2)}) async-start(), calls=%async_computation | async-start | bytes 7077888 | tf_op jit(solution)/shard_map/all_gather | solution.py:256
  7.5 155.6 %copy-start.3 = (bf16[1,192,512]{2,1,0:T(8,128)(2,1)S(1)}, bf16[1,192,512]{2,1,0:T(8,128)(2,1)}, u32[]{:S(2)}) copy-start(bf16[1,192,512]{2,1,0:T(8,128)(2,1)} %param.10) | copy-start | bytes 589828
  28.4 0.7 collective-permute-start
  46.5 24.9 %collective-permute-start.1 = (bf16[256,1536]{1,0:T(8,128)(2,1)S(1)}, bf16[256,1536]{1,0:T(8,128)(2,1)S(1)}, u32[]{:S(2)}, u32[]{:S(2)}) collective-permute-start(bf16[256,1536]{1,0:T(8,128)(2,1)S(1)} %all_gather.38.rest_0_), channel_id=1, source_target_pairs={{0,896},{128,0},{256,128},{384,256},{512,384},{640,512},{768,640},... | collective-permute-start | bytes 2359304 | tf_op jit(solution)/shard_map/ppermute | solution.py:217
  59.4 20.8 %collective-permute-start.2 = (bf16[256,1536]{1,0:T(8,128)(2,1)S(1)}, bf16[256,1536]{1,0:T(8,128)(2,1)S(1)}, u32[]{:S(2)}, u32[]{:S(2)}) collective-permute-start(bf16[256,1536]{1,0:T(8,128)(2,1)S(1)} %all_gather.38.rest_0_), channel_id=1, source_target_pairs={{0,128},{128,256},{256,384},{384,512},{512,640},{640,768},{768,896... | collective-permute-start | bytes 2359304 | tf_op jit(solution)/shard_map/ppermute | solution.py:217
  71.4 29.5 %collective-permute-start.3 = (bf16[256,1536]{1,0:T(8,128)(2,1)S(1)}, bf16[256,1536]{1,0:T(8,128)(2,1)S(1)}, u32[]{:S(2)}, u32[]{:S(2)}) collective-permute-start(bf16[256,1536]{1,0:T(8,128)(2,1)S(1)} %collective-permute-done.1.rest_1_), channel_id=1, source_target_pairs={{0,896},{128,0},{256,128},{384,256},{512,384},{640,512},{768,640},... | collective-permute-start | bytes 2359304 | tf_op jit(solution)/shard_map/ppermute | solution.py:217
  80.3 38.5 %collective-permute-start.5 = (bf16[256,1536]{1,0:T(8,128)(2,1)S(1)}, bf16[256,1536]{1,0:T(8,128)(2,1)}, u32[]{:S(2)}, u32[]{:S(2)}) collective-permute-start(bf16[256,1536]{1,0:T(8,128)(2,1)S(1)} %collective-permute-done.2.rest_2_), channel_id=1, source_target_pairs={{0,128},{128,256},{256,384},{384,512},{512,640},{640,768},{768,896... | collective-permute-start | bytes 2359304 | tf_op jit(solution)/shard_map/ppermute | solution.py:217
  100.9 27.8 %collective-permute-start.4 = (bf16[256,1536]{1,0:T(8,128)(2,1)S(1)}, bf16[256,1536]{1,0:T(8,128)(2,1)}, u32[]{:S(2)}, u32[]{:S(2)}) collective-permute-start(bf16[256,1536]{1,0:T(8,128)(2,1)S(1)} %collective-permute-done.3.rest_3_), channel_id=1, source_target_pairs={{0,896},{128,0},{256,128},{384,256},{512,384},{640,512},{768,640},... | collective-permute-start | bytes 2359304 | tf_op jit(solution)/shard_map/ppermute | solution.py:217
  115.5 0.9 copy-start
  116.4 0.9 copy-start.2
  117.3 0.7 copy-start.4
  118.0 0.7 copy-start.5
  118.7 54.1 %collective-permute-start.7 = (bf16[256,1536]{1,0:T(8,128)(2,1)}, bf16[256,1536]{1,0:T(8,128)(2,1)}, u32[]{:S(2)}, u32[]{:S(2)}) collective-permute-start(bf16[256,1536]{1,0:T(8,128)(2,1)} %collective-permute-done.5.rest_5_), channel_id=1, source_target_pairs={{0,128},{128,256},{256,384},{384,512},{512,640},{640,768},{768,896... | collective-permute-start | bytes 2359304 | tf_op jit(solution)/shard_map/ppermute | solution.py:217
  128.8 44.1 %collective-permute-start.6 = (bf16[256,1536]{1,0:T(8,128)(2,1)}, bf16[256,1536]{1,0:T(8,128)(2,1)}, u32[]{:S(2)}, u32[]{:S(2)}) collective-permute-start(bf16[256,1536]{1,0:T(8,128)(2,1)} %collective-permute-done.4.rest_4_), channel_id=1, source_target_pairs={{0,896},{128,0},{256,128},{384,256},{512,384},{640,512},{768,640},... | collective-permute-start | bytes 2359304 | tf_op jit(solution)/shard_map/ppermute | solution.py:217
  154.2 18.6 %copy-start.1 = (bf16[256,1536]{1,0:T(8,128)(2,1)S(1)}, bf16[256,1536]{1,0:T(8,128)(2,1)}, u32[]{:S(2)}) copy-start(bf16[256,1536]{1,0:T(8,128)(2,1)} %copy-done) | copy-start | bytes 2359300
  194.5 16.4 %copy-start.6 = (f32[512]{0:T(512)S(1)}, f32[512]{0:T(512)}, u32[]{:S(2)}) copy-start(f32[512]{0:T(512)} %param.19) | copy-start | bytes 6148
Sparse Core Ops, SparseCore 0:
  27.6 89.6 all-gather.3
where the time goes:
time: 219 us
  blocking collectives  104 us (47%)
  starting transfers between devices  54.3 us (25%)
  waiting for transfers between devices  30.9 us (14%)
  between operations  13.6 us (6%)
  Pallas kernels  9.87 us (5%)
  local copies, waits for them, and re-layouts  3.27 us (1%)
  other arithmetic  2.71 us (1%)
    all_gather x6, blocking collectives, _whole(): return lax.all_gather(local_rows, ('xl', 'co'), axis=1, tiled=True)  61.5 us
    ppermute x7, starting transfers between devices, _shift(): return lax.ppermute(value, axis, [(i, (i + by) % n) for i in range(n)])  53.6 us
    all_gather x2, blocking collectives, _over_xh(): return lax.all_gather(value, 'xh', axis=0, tiled=True)  37.4 us
    ppermute x7, waiting for transfers between devices, _shift(): return lax.ppermute(value, axis, [(i, (i + by) % n) for i in range(n)])  30.8 us
    pallas_call x7, Pallas kernels, _call(): pl.pallas_call(kernel, out_shape=outs, in_specs=[full] * len(args) + [far...  9.87 us
    all_gather x1, blocking collectives, shards(): every = lax.all_gather(stats[:, :2].T, ('xl', 'co'), axis=0, tiled=False)  5.18 us
  transfers between devices with their start and end apart: 9, of which 4 were waited for; matrix products, arithmetic and copies ran while one was open for 0% of the time, Pallas kernels for 2%

commit v1 on v0

--- a/solution.py
+++ b/solution.py
@@ -15,7 +15,7 @@
 SEQ = 192
 D = 2048
 LOC = 512
-ROWS = 208
+ROWS = 200
 NZ = 8
 NX = 4
 KB = 256
@@ -69,22 +69,21 @@
     width = 2 * 128
     token = lax.broadcasted_iota(jnp.int32, (SEQ, width), 0)
     lane = lax.broadcasted_iota(jnp.int32, (SEQ, width), 1)
-    cents, sums = [], None
+    cents, locals_, inner = [], [], None
     for j in range(4):
         zc = pay_ref[:SEQ, j * LOC : (j + 1) * LOC].astype(F32)
         terms = pay_ref[SEQ:, j * LOC : j * LOC + width].astype(F32)
         across = jnp.sum(terms, axis=0, keepdims=True)
         cent = jnp.sum(jnp.where(token == lane, across, 0.0), axis=1, keepdims=True)
-        s = jnp.sum(zc, axis=1, keepdims=True) + LOC * cent
-        sums = s if sums is None else sums + s
+        rest = jnp.sum(zc, axis=1, keepdims=True) / LOC
+        square = jnp.sum(zc * zc, axis=1, keepdims=True) - LOC * rest * rest
+        inner = square if inner is None else inner + square
         cents.append(cent)
-    mean = sums / D
-    var = None
-    for j in range(4):
-        zc = pay_ref[:SEQ, j * LOC : (j + 1) * LOC].astype(F32)
-        dev = zc + (cents[j] - mean)
-        v = jnp.sum(dev * dev, axis=1, keepdims=True)
-        var = v if var is None else var + v
+        locals_.append(cent + rest)
+    mean = (locals_[0] + locals_[1] + locals_[2] + locals_[3]) / 4
+    var = inner
+    for local in locals_:
+        var = var + LOC * (local - mean) * (local - mean)
     scale = lax.rsqrt(var / D + norm_eps)
     for j in range(4):
         zc = pay_ref[:SEQ, j * LOC : (j + 1) * LOC].astype(F32)

time: 219 us -> 219 us (level)
  no operation moved by 1% of the time
where the time goes in v1:
time: 219 us; the launch traced here: 218 us
  blocking collectives  104 us (47%)
  starting transfers between devices  54.3 us (25%)
  waiting for transfers between devices  30.9 us (14%)
  between operations  13.6 us (6%)
  Pallas kernels  9.71 us (4%)
  local copies, waits for them, and re-layouts  3.27 us (1%)
  other arithmetic  2.71 us (1%)
    all_gather x6, blocking collectives, _whole(): return lax.all_gather(local_rows, ('xl', 'co'), axis=1, tiled=True)  61 us
    ppermute x7, starting transfers between devices, _shift(): return lax.ppermute(value, axis, [(i, (i + by) % n) for i in range(n)])  53.6 us
    all_gather x2, blocking collectives, _over_xh(): return lax.all_gather(value, 'xh', axis=0, tiled=True)  37.4 us
    ppermute x7, waiting for transfers between devices, _shift(): return lax.ppermute(value, axis, [(i, (i + by) % n) for i in range(n)])  30.8 us
    pallas_call x7, Pallas kernels, _call(): pl.pallas_call(kernel, out_shape=outs, in_specs=[full] * len(args) + [far...  9.71 us
    all_gather x1, blocking collectives, shards(): every = lax.all_gather(stats[:, :2].T, ('xl', 'co'), axis=0, tiled=False)  5.18 us
  transfers between devices with their start and end apart: 9, of which 4 were waited for; matrix products, arithmetic and copies ran while one was open for 0% of the time, Pallas kernels for 2%

profile of v1, /device:TPU:129, one launch (start us, length us, event | category | flops | bytes accessed | tf_op | source)
XLA Modules:
  0.0 217.9 jit_solution(17063382374729128550)
XLA Ops:
  6.5 0.9 pad_maximum_fusion
  7.5 20.0 %all_gather.34 = bf16[256,1536]{1,0:T(8,128)(2,1)} all-gather(bf16[64,1536]{1,0:T(8,128)(2,1)S(1)} %pad_maximum_fusion), channel_id=1, replica_groups=mesh['rep'=8,'z'=8,'xh'=4,'xl'=2,'co'=2] {'xh'}, dimensions={0}, use_global_device_ids=true | all-gather | bytes 983040 | tf_op jit(solution)/shard_map/all_gather | solution.py:229
  27.5 0.9 pad_maximum_fusion.1
  29.1 17.4 %all_gather.38.rest_0_ = bf16[256,1536]{1,0:T(8,128)(2,1)S(1)} all-gather(bf16[64,1536]{1,0:T(8,128)(2,1)S(1)} %collective-permute-done), channel_id=1, replica_groups=mesh['rep'=8,'z'=8,'xh'=4,'xl'=2,'co'=2] {'xh'}, dimensions={0}, use_global_device_ids=true | all-gather | bytes 983040 | tf_op jit(solution)/shard_map/all_gather | solution.py:229
  46.5 12.9 %collective-permute-start.1 = (bf16[256,1536]{1,0:T(8,128)(2,1)S(1)}, bf16[256,1536]{1,0:T(8,128)(2,1)S(1)}, u32[]{:S(2)}, u32[]{:S(2)}) collective-permute-start(bf16[256,1536]{1,0:T(8,128)(2,1)S(1)} %all_gather.38.rest_0_), channel_id=1, source_target_pairs={{0,896},{128,0},{256,128},{384,256},{512,384},{640,512},{768,640},... | collective-permute-start | bytes 2359304 | tf_op jit(solution)/shard_map/ppermute | solution.py:216
  59.4 1.9 collective-permute-start.2
  61.4 10.1 %collective-permute-done.1.rest_1_ = bf16[256,1536]{1,0:T(8,128)(2,1)S(1)} collective-permute-done((bf16[256,1536]{1,0:T(8,128)(2,1)S(1)}, bf16[256,1536]{1,0:T(8,128)(2,1)S(1)}, u32[]{:S(2)}, u32[]{:S(2)}) %collective-permute-start.1) | collective-permute-done | bytes 786464 | tf_op jit(solution)/shard_map/ppermute | solution.py:216
  71.4 8.4 %collective-permute-start.3 = (bf16[256,1536]{1,0:T(8,128)(2,1)S(1)}, bf16[256,1536]{1,0:T(8,128)(2,1)S(1)}, u32[]{:S(2)}, u32[]{:S(2)}) collective-permute-start(bf16[256,1536]{1,0:T(8,128)(2,1)S(1)} %collective-permute-done.1.rest_1_), channel_id=1, source_target_pairs={{0,896},{128,0},{256,128},{384,256},{512,384},{640,512},{768,640},... | collective-permute-start | bytes 2359304 | tf_op jit(solution)/shard_map/ppermute | solution.py:216
  80.3 8.4 %collective-permute-start.5 = (bf16[256,1536]{1,0:T(8,128)(2,1)S(1)}, bf16[256,1536]{1,0:T(8,128)(2,1)}, u32[]{:S(2)}, u32[]{:S(2)}) collective-permute-start(bf16[256,1536]{1,0:T(8,128)(2,1)S(1)} %collective-permute-done.2.rest_2_), channel_id=1, source_target_pairs={{0,128},{128,256},{256,384},{384,512},{512,640},{640,768},{768,896... | collective-permute-start | bytes 2359304 | tf_op jit(solution)/shard_map/ppermute | solution.py:216
  88.7 12.2 %collective-permute-done.3.rest_3_ = bf16[256,1536]{1,0:T(8,128)(2,1)S(1)} collective-permute-done((bf16[256,1536]{1,0:T(8,128)(2,1)S(1)}, bf16[256,1536]{1,0:T(8,128)(2,1)S(1)}, u32[]{:S(2)}, u32[]{:S(2)}) %collective-permute-start.3) | collective-permute-done | bytes 786464 | tf_op jit(solution)/shard_map/ppermute | solution.py:216
  100.9 14.6 %collective-permute-start.4 = (bf16[256,1536]{1,0:T(8,128)(2,1)S(1)}, bf16[256,1536]{1,0:T(8,128)(2,1)}, u32[]{:S(2)}, u32[]{:S(2)}) collective-permute-start(bf16[256,1536]{1,0:T(8,128)(2,1)S(1)} %collective-permute-done.3.rest_3_), channel_id=1, source_target_pairs={{0,896},{128,0},{256,128},{384,256},{512,384},{640,512},{768,640},... | collective-permute-start | bytes 2359304 | tf_op jit(solution)/shard_map/ppermute | solution.py:216
  115.5 0.9 copy-done
  116.4 0.9 copy-done.2
  117.3 0.7 copy-done.4
  118.0 0.7 copy-done.5
  118.7 1.9 collective-permute-start.7
  120.7 8.1 %collective-permute-done.4.rest_4_ = bf16[256,1536]{1,0:T(8,128)(2,1)} collective-permute-done((bf16[256,1536]{1,0:T(8,128)(2,1)S(1)}, bf16[256,1536]{1,0:T(8,128)(2,1)}, u32[]{:S(2)}, u32[]{:S(2)}) %collective-permute-start.4) | collective-permute-done | bytes 786464 | tf_op jit(solution)/shard_map/ppermute | solution.py:216
  128.8 5.4 %collective-permute-start.6 = (bf16[256,1536]{1,0:T(8,128)(2,1)}, bf16[256,1536]{1,0:T(8,128)(2,1)}, u32[]{:S(2)}, u32[]{:S(2)}) collective-permute-start(bf16[256,1536]{1,0:T(8,128)(2,1)} %collective-permute-done.4.rest_4_), channel_id=1, source_target_pairs={{0,896},{128,0},{256,128},{384,256},{512,384},{640,512},{768,640},... | collective-permute-start | bytes 2359304 | tf_op jit(solution)/shard_map/ppermute | solution.py:216
  134.2 16.9 %all_gather.33.tok_ref = bf16[200,2048]{1,0:T(8,128)(2,1)S(1)} all-gather(bf16[200,512]{1,0:T(8,128)(2,1)S(1)} %shard_map.100), channel_id=1, replica_groups=mesh['rep'=8,'z'=8,'xh'=4,'xl'=2,'co'=2] {'xl','co'}, dimensions={1}, use_global_device_ids=true | all-gather | bytes 1024000 | tf_op jit(solution)/shard_map/all_gather | solution.py:246
  151.1 2.9 %shard_map.101 = (bf16[192,512]{1,0:T(8,128)(2,1)S(1)}, bf16[2048,1536]{1,0:T(8,128)(2,1)S(1)}) custom-call(bf16[200,2048]{1,0:T(8,128)(2,1)S(1)} %all_gather.33.tok_ref, bf16[2048,1536]{1,0:T(8,128)(2,1)} %all-gather.4.cloned.1.call-done.w_ref), custom_call_target="tpu_custom_call" | custom-call | flops 805306368 | bytes 7110656 | tf_op jit(solution)/shard_map/pallas_call | solution.py:179
  154.1 8.8 %all_gather.36.hid_ref = bf16[192,2048]{1,0:T(8,128)(2,1)S(1)} all-gather(bf16[192,512]{1,0:T(8,128)(2,1)S(1)} %get-tuple-element.14), channel_id=1, replica_groups=mesh['rep'=8,'z'=8,'xh'=4,'xl'=2,'co'=2] {'xl','co'}, dimensions={1}, use_global_device_ids=true | all-gather | bytes 983040 | tf_op jit(solution)/shard_map/all_gather | solution.py:246
  162.9 0.7 shard_map.102
  163.6 8.9 %all_gather.37.pay_ref = bf16[200,2048]{1,0:T(8,128)(2,1)S(1)} all-gather(bf16[200,512]{1,0:T(8,128)(2,1)S(1)} %shard_map.102), channel_id=1, replica_groups=mesh['rep'=8,'z'=8,'xh'=4,'xl'=2,'co'=2] {'xl','co'}, dimensions={1}, use_global_device_ids=true | all-gather | bytes 1024000 | tf_op jit(solution)/shard_map/all_gather | solution.py:246
  172.5 3.2 %shard_map.103 = (bf16[192,512]{1,0:T(8,128)(2,1)S(1)}, bf16[192,512]{1,0:T(8,128)(2,1)S(1)}, bf16[4,256,1536]{2,1,0:T(8,128)(2,1)S(1)}) custom-call(bf16[200,2048]{1,0:T(8,128)(2,1)S(1)} %all_gather.37.pay_ref, bf16[8,2048]{1,0:T(8,128)(2,1)S(1)} %slice.16.gain_ref, bf16[256,1536]{1,0:T(8,128)(2,1)S(1)} %all_gather.38.rest_0_, ...), custom_call_target="tpu_custom_call" | custom-call | flops 805306368 | bytes 7143424 | tf_op jit(solution)/shard_map/pallas_call | solution.py:179
  175.7 8.7 %all_gather.39.hid_ref = bf16[192,2048]{1,0:T(8,128)(2,1)S(1)} all-gather(bf16[192,512]{1,0:T(8,128)(2,1)S(1)} %get-tuple-element.16), channel_id=1, replica_groups=mesh['rep'=8,'z'=8,'xh'=4,'xl'=2,'co'=2] {'xl','co'}, dimensions={1}, use_global_device_ids=true | all-gather | bytes 983040 | tf_op jit(solution)/shard_map/all_gather | solution.py:246
  184.4 0.7 shard_map.104
  185.1 8.9 %all_gather.40.pay_ref = bf16[200,2048]{1,0:T(8,128)(2,1)S(1)} all-gather(bf16[200,512]{1,0:T(8,128)(2,1)S(1)} %shard_map.104), channel_id=1, replica_groups=mesh['rep'=8,'z'=8,'xh'=4,'xl'=2,'co'=2] {'xl','co'}, dimensions={1}, use_global_device_ids=true | all-gather | bytes 1024000 | tf_op jit(solution)/shard_map/all_gather | solution.py:246
  194.0 1.4 shard_map.105
  195.4 8.7 %all_gather.41.hid_ref = bf16[192,2048]{1,0:T(8,128)(2,1)S(1)} all-gather(bf16[192,512]{1,0:T(8,128)(2,1)S(1)} %get-tuple-element.19), channel_id=1, replica_groups=mesh['rep'=8,'z'=8,'xh'=4,'xl'=2,'co'=2] {'xl','co'}, dimensions={1}, use_global_device_ids=true | all-gather | bytes 983040 | tf_op jit(solution)/shard_map/all_gather | solution.py:246
  204.2 0.7 shard_map.106
  205.0 5.2 %all-gather.1 = f32[4,2,192]{2,1,0:T(2,128)S(1)} all-gather(f32[1,2,192]{2,1,0:T(2,128)S(1)} %copy.11), channel_id=2, replica_groups=mesh['rep'=8,'z'=8,'xh'=4,'xl'=2,'co'=2] {'xl','co'}, dimensions={0}, use_global_device_ids=true | all-gather | bytes 7680 | tf_op jit(solution)/shard_map/all_gather | solution.py:285
  210.3 0.8 fusion
  (27 shorter events, 1.4 us)
Async XLA Ops:
  6.5 144.6 %all-gather.4.cloned.1.call-start = ((), (), s32[]{:S(2)}) async-start(), calls=%async_computation | async-start | bytes 7077888 | tf_op jit(solution)/shard_map/all_gather | solution.py:255
  7.5 155.4 %copy-start.3 = (bf16[1,192,512]{2,1,0:T(8,128)(2,1)S(1)}, bf16[1,192,512]{2,1,0:T(8,128)(2,1)}, u32[]{:S(2)}) copy-start(bf16[1,192,512]{2,1,0:T(8,128)(2,1)} %param.10) | copy-start | bytes 589828
  28.4 0.7 collective-permute-start
  46.5 24.9 %collective-permute-start.1 = (bf16[256,1536]{1,0:T(8,128)(2,1)S(1)}, bf16[256,1536]{1,0:T(8,128)(2,1)S(1)}, u32[]{:S(2)}, u32[]{:S(2)}) collective-permute-start(bf16[256,1536]{1,0:T(8,128)(2,1)S(1)} %all_gather.38.rest_0_), channel_id=1, source_target_pairs={{0,896},{128,0},{256,128},{384,256},{512,384},{640,512},{768,640},... | collective-permute-start | bytes 2359304 | tf_op jit(solution)/shard_map/ppermute | solution.py:216
  59.4 20.8 %collective-permute-start.2 = (bf16[256,1536]{1,0:T(8,128)(2,1)S(1)}, bf16[256,1536]{1,0:T(8,128)(2,1)S(1)}, u32[]{:S(2)}, u32[]{:S(2)}) collective-permute-start(bf16[256,1536]{1,0:T(8,128)(2,1)S(1)} %all_gather.38.rest_0_), channel_id=1, source_target_pairs={{0,128},{128,256},{256,384},{384,512},{512,640},{640,768},{768,896... | collective-permute-start | bytes 2359304 | tf_op jit(solution)/shard_map/ppermute | solution.py:216
  71.4 29.5 %collective-permute-start.3 = (bf16[256,1536]{1,0:T(8,128)(2,1)S(1)}, bf16[256,1536]{1,0:T(8,128)(2,1)S(1)}, u32[]{:S(2)}, u32[]{:S(2)}) collective-permute-start(bf16[256,1536]{1,0:T(8,128)(2,1)S(1)} %collective-permute-done.1.rest_1_), channel_id=1, source_target_pairs={{0,896},{128,0},{256,128},{384,256},{512,384},{640,512},{768,640},... | collective-permute-start | bytes 2359304 | tf_op jit(solution)/shard_map/ppermute | solution.py:216
  80.3 38.5 %collective-permute-start.5 = (bf16[256,1536]{1,0:T(8,128)(2,1)S(1)}, bf16[256,1536]{1,0:T(8,128)(2,1)}, u32[]{:S(2)}, u32[]{:S(2)}) collective-permute-start(bf16[256,1536]{1,0:T(8,128)(2,1)S(1)} %collective-permute-done.2.rest_2_), channel_id=1, source_target_pairs={{0,128},{128,256},{256,384},{384,512},{512,640},{640,768},{768,896... | collective-permute-start | bytes 2359304 | tf_op jit(solution)/shard_map/ppermute | solution.py:216
  100.9 27.8 %collective-permute-start.4 = (bf16[256,1536]{1,0:T(8,128)(2,1)S(1)}, bf16[256,1536]{1,0:T(8,128)(2,1)}, u32[]{:S(2)}, u32[]{:S(2)}) collective-permute-start(bf16[256,1536]{1,0:T(8,128)(2,1)S(1)} %collective-permute-done.3.rest_3_), channel_id=1, source_target_pairs={{0,896},{128,0},{256,128},{384,256},{512,384},{640,512},{768,640},... | collective-permute-start | bytes 2359304 | tf_op jit(solution)/shard_map/ppermute | solution.py:216
  115.5 0.9 copy-start
  116.4 0.9 copy-start.2
  117.3 0.7 copy-start.4
  118.0 0.7 copy-start.5
  118.7 53.7 %collective-permute-start.7 = (bf16[256,1536]{1,0:T(8,128)(2,1)}, bf16[256,1536]{1,0:T(8,128)(2,1)}, u32[]{:S(2)}, u32[]{:S(2)}) collective-permute-start(bf16[256,1536]{1,0:T(8,128)(2,1)} %collective-permute-done.5.rest_5_), channel_id=1, source_target_pairs={{0,128},{128,256},{256,384},{384,512},{512,640},{640,768},{768,896... | collective-permute-start | bytes 2359304 | tf_op jit(solution)/shard_map/ppermute | solution.py:216
  128.8 43.7 %collective-permute-start.6 = (bf16[256,1536]{1,0:T(8,128)(2,1)}, bf16[256,1536]{1,0:T(8,128)(2,1)}, u32[]{:S(2)}, u32[]{:S(2)}) collective-permute-start(bf16[256,1536]{1,0:T(8,128)(2,1)} %collective-permute-done.4.rest_4_), channel_id=1, source_target_pairs={{0,896},{128,0},{256,128},{384,256},{512,384},{640,512},{768,640},... | collective-permute-start | bytes 2359304 | tf_op jit(solution)/shard_map/ppermute | solution.py:216
  154.1 18.4 %copy-start.1 = (bf16[256,1536]{1,0:T(8,128)(2,1)S(1)}, bf16[256,1536]{1,0:T(8,128)(2,1)}, u32[]{:S(2)}) copy-start(bf16[256,1536]{1,0:T(8,128)(2,1)} %copy-done) | copy-start | bytes 2359300
  194.0 16.3 %copy-start.6 = (f32[512]{0:T(512)S(1)}, f32[512]{0:T(512)}, u32[]{:S(2)}) copy-start(f32[512]{0:T(512)} %param.19) | copy-start | bytes 6148
Sparse Core Ops, SparseCore 0:
  27.6 89.6 all-gather.3
